TPU v7x, 32 devices: a whole 2x2x4 slice. The times are simulated.
32 devices in a mesh: sp: 8 (over z, y), tp: 4 (over x, core).
Axes of the slice: x: 2, y: 2, z: 4, core: 2. Of those that a mesh axis runs over, the one named last changes fastest.
Arguments:
- glu_value: bfloat16 [4096, 2048], P('sp', 'tp'), may hold values from -640 to 640
- glu_gate: bfloat16 [4096, 2048], P('sp', 'tp'), may hold values from -9 to 9
- conv_kernel: float32 [31, 2048], P(None, 'tp'), may hold values from -1 to 1
- norm_gain: float32 [2048], P('tp'), may hold values from 0.1 to 1.9
- mix_weight: bfloat16 [2048, 2048], P('tp'), may hold values from -0.125 to 0.125
- residual: bfloat16 [4096, 2048], P(('sp', 'tp')), may hold values from -6 to 6
- resid_gain: float32 [2048], replicated, may hold values from 0.1 to 1.9
- expert_ids: int32 [4096, 2], P(('sp', 'tp')), may hold values from 0 to 7, all different within a row; in each aligned block of 128 rows (0 to 127, 128 to 255, ...) at most 64 rows name the same one
- route_weight: float32 [4096, 2], P(('sp', 'tp')), may hold values from 0.05 to 0.5
- w_gate: bfloat16 [8, 2048, 2048], P('sp', None, 'tp'), may hold values from -0.5 to 0.5
- w_up: bfloat16 [8, 2048, 2048], P('sp', None, 'tp'), may hold values from -0.5 to 0.5
- w_down: bfloat16 [8, 2048, 2048], P('sp', 'tp'), may hold values from -0.03125 to 0.03125
- out_gain: float32 [2048], replicated, may hold values from 0.1 to 1.9
Outputs:
- blended: bfloat16 [4096, 2048], P(('sp', 'tp'))
Inputs may be any that keep to these rules, and one draw needn't show every extreme that they name: `expert_ids`: in each aligned block of 128 rows (the rows of one device) no expert is named by more than 64 rows, a bound that some block reaches.
All inputs are finite; a program needn't handle non-finite values.
Results may differ from a plain program's by a relative error of at most 0.015.
Values may be sent and summed in bfloat16 or wider, within the bound.
A program may use at most 128 MiB of HBM per device.

v0:
```python
import jax
import jax.numpy as jnp
from jax import lax
from jax.sharding import PartitionSpec as P

DC = 2048


EPSILON = 1e-05
LIMIT = 7.0
SLOPE = 1.702


def shifted(block, axis, distance):
    devices = range(lax.axis_size(axis))
    route = [(i - distance, i) for i in devices if i - distance in devices]
    return lax.ppermute(block, axis, route)


def normalize(values, gain_vector):
    centre = jnp.mean(values, axis=-1, keepdims=True)
    spread = jnp.mean(jnp.square(values - centre), axis=-1, keepdims=True)
    return (values - centre) * lax.rsqrt(spread + EPSILON) * gain_vector


def slot_layout(route_ids, experts, capacity):
    row_count, top_count = route_ids.shape
    flat_ids = route_ids.reshape(row_count * top_count)
    onehot = (flat_ids[:, None] == jnp.arange(experts, dtype=jnp.int32)[None, :]).astype(jnp.int32)
    before = jnp.cumsum(onehot, axis=0) - onehot
    slot_rank = jnp.sum(before * onehot, axis=1)
    position = flat_ids * capacity + slot_rank
    owners = jnp.arange(row_count * top_count, dtype=jnp.int32) // top_count
    slot_table = jnp.full((experts * capacity,), row_count, jnp.int32).at[position].set(owners)
    return (slot_table, position.reshape(row_count, top_count))


def expert_activity(tokens, gate_matrix, up_matrix):
    gate_pre = jnp.dot(tokens, gate_matrix, preferred_element_type=jnp.float32)
    up_pre = jnp.dot(tokens, up_matrix, preferred_element_type=jnp.float32)
    gated = jnp.minimum(gate_pre, LIMIT)
    upper = jnp.clip(up_pre, -LIMIT, LIMIT)
    return ((upper + 1.0) * gated * jax.nn.sigmoid(SLOPE * gated)).astype(jnp.bfloat16)


def shards(
    glu_value,
    glu_gate,
    conv_kernel,
    norm_gain,
    mix_weight,
    residual,
    resid_gain,
    expert_ids,
    route_weight,
    w_gate,
    w_up,
    w_down,
    out_gain,
):
    gated_in = (
        glu_value.astype(jnp.float32) * jax.nn.sigmoid(glu_gate.astype(jnp.float32))
    ).astype(jnp.bfloat16)
    reach_back = conv_kernel.shape[0] - 1
    length = gated_in.shape[0]
    before_rows = shifted(gated_in[length - reach_back :], "sp", 1)
    extended = jnp.concatenate([before_rows, gated_in], axis=0).astype(jnp.float32)
    convolved = jnp.zeros(gated_in.shape, jnp.float32)
    for offset in range(reach_back + 1):
        convolved = convolved + conv_kernel[offset] * extended[offset : offset + length]
    channel_sum, squares = lax.psum(
        (jnp.sum(convolved, axis=1), jnp.sum(convolved * convolved, axis=1)), "tp"
    )
    centre = channel_sum / DC
    spread = squares / DC - centre * centre
    normed = (convolved - centre[:, None]) * lax.rsqrt(spread[:, None] + EPSILON) * norm_gain
    mix_in = jax.nn.silu(normed).astype(jnp.bfloat16)
    tp_count = lax.axis_size("tp")
    own_count = length // tp_count
    section = mix_in
    mixed_rows = lax.psum_scatter(
        jnp.dot(section, mix_weight, preferred_element_type=jnp.float32).astype(jnp.bfloat16),
        "tp",
        scatter_dimension=0,
        tiled=True,
    ).astype(jnp.float32)
    hidden = normalize(residual.astype(jnp.float32) + mixed_rows, resid_gain).astype(jnp.bfloat16)
    experts = lax.axis_size("sp")
    top_count = expert_ids.shape[1]
    capacity = 2 * own_count * top_count // experts
    width = hidden.shape[1]
    gate_local = w_gate[0]
    up_local = w_up[0]
    down_local = w_down[0]
    own_table, positions = slot_layout(expert_ids, experts, capacity)
    padded = jnp.concatenate([hidden, jnp.zeros((1, width), jnp.bfloat16)], axis=0)
    dispatched = padded[own_table].reshape(experts, capacity, width)
    arrived = lax.all_to_all(dispatched, "sp", split_axis=0, concat_axis=0, tiled=True)
    activate_arrived = lax.all_gather(arrived[None], "tp", axis=0, tiled=True)
    arrived_shape = activate_arrived.shape
    flat_rows = activate_arrived.reshape(-1, arrived_shape[-1])
    activity = expert_activity(flat_rows, gate_local, up_local)
    activity = activity.reshape(arrived_shape[:-1] + (gate_local.shape[1],))
    activity_rows = activity.reshape(-1, activity.shape[-1])
    section = activity_rows
    expert_out = lax.psum_scatter(
        jnp.dot(section, down_local, preferred_element_type=jnp.float32).astype(jnp.bfloat16),
        "tp",
        scatter_dimension=0,
        tiled=True,
    )
    expert_out = expert_out.reshape(experts, capacity, width)
    returned_rows = lax.all_to_all(expert_out, "sp", split_axis=0, concat_axis=0, tiled=True)
    picked = returned_rows.reshape(experts * capacity, width)[positions.reshape(-1)]
    picked = picked.reshape(own_count, top_count, width)
    routed_sum = jnp.einsum("tk,tkd->td", route_weight, picked.astype(jnp.float32))
    return normalize(hidden.astype(jnp.float32) + routed_sum, out_gain).astype(jnp.bfloat16)


def solution(mesh):
    in_specs = (
        P("sp", "tp"),
        P("sp", "tp"),
        P(None, "tp"),
        P("tp"),
        P("tp", None),
        P(("sp", "tp"), None),
        P(),
        P(("sp", "tp"), None),
        P(("sp", "tp"), None),
        P("sp", None, "tp"),
        P("sp", None, "tp"),
        P("sp", "tp", None),
        P(),
    )
    out_specs = P(("sp", "tp"), None)
    return jax.shard_map(shards, mesh=mesh, in_specs=in_specs, out_specs=out_specs, check_vma=False)
```

profile of v0, /device:TPU:0, one launch (start us, length us, event | category | flops | bytes accessed | tf_op | source)
XLA Modules:
  0.0 345.0 jit_solution(18166377911452001083)
XLA Ops:
  6.5 0.0 copy-start
  6.5 0.0 reduce-scatter.3.cloned.1.call-start
  6.5 1.6 multiply_convert_fusion.4
  8.2 4.9 %collective-permute-start = (bf16[30,512]{1,0:T(8,128)(2,1)S(1)}, bf16[30,512]{1,0:T(8,128)(2,1)S(1)}, u32[]{:S(2)}, u32[]{:S(2)}) collective-permute-start(bf16[30,512]{1,0:T(8,128)(2,1)S(1)} %slice.264), channel_id=1, source_target_pairs={{0,4},{4,8},{8,12},{12,16},{16,20},{20,24},{24,28},{1,5},{5,9},{9,... | collective-permute-start | bytes 92168 | tf_op jit(solution)/shard_map/ppermute | solution.py:17
  13.1 1.2 fusion.49
  14.3 1.0 fusion.50
  15.3 0.0 collective-permute-done
  15.3 0.2 maximum_convert_fusion
  15.5 0.0 copy-start.9
  15.5 5.0 %fusion.47 = (f32[512]{0:T(512)S(1)}, f32[512]{0:T(512)S(1)}, f32[512,512]{1,0:T(8,128)S(1)}) fusion(f32[542,512]{1,0:T(8,128)S(1)} %maximum_convert_fusion, f32[512]{0:T(512)S(1)} %bitcast.100, f32[512]{0:T(512)S(1)} %bitcast.101, f32[512]{0:T(512)S(1)} %bitcast.72, f32[512]{0:T(512)S(1)} %bitcast.73, f32[512]{0:T(512)S(1)} %bitcast.74, ...), kind=kLoop, calls=%fused_computation.113 | loop fusion | flops 16776192 | bytes 33622016 | tf_op jit(solution)/shard_map/reduce_sum | solution.py:72
  20.5 6.3 %all-reduce.1 = (f32[512]{0:T(512)S(1)}, f32[512]{0:T(512)S(1)}) all-reduce(f32[512]{0:T(512)S(1)} %get-tuple-element.6, f32[512]{0:T(512)S(1)} %get-tuple-element.5), channel_id=1, replica_groups=mesh['sp'=8,'tp'=4] {'tp'}, use_global_device_ids=true, to_apply=%region_3.0 | all-reduce | flops 1024 | bytes 8192 | tf_op jit(solution)/shard_map/psum | solution.py:71
  26.8 0.0 copy-done.9
  26.8 4.4 %convolution_convert_fusion.1 = bf16[512,2048]{1,0:T(8,128)(2,1)} fusion(bf16[512,2048]{1,0:T(8,128)(2,1)} %param.17, f32[512,512]{1,0:T(8,128)S(1)} %get-tuple-element.9, f32[512]{0:T(512)S(1)} %copy-done.9, f32[512]{0:T(512)S(1)} %get-tuple-element.42, f32[512]{0:T(512)S(1)} %get-tuple-element.41), kind=kOutput, calls=%fused_computation.5 | convolution fusion | flops 1076887552 | bytes 5249024 | tf_op jit(solution)/shard_map/dot_general | solution.py:82
  31.3 0.0 copy-start.5
  31.3 0.0 copy-start.1
  31.3 0.0 copy-start.3
  31.3 0.0 reduce-scatter.3.cloned.1.call-update
  31.3 0.0 all-gather.3.cloned.1.call-start
  31.3 0.6 copy-done.5
  31.9 0.1 copy.18
  32.1 0.1 eq.29
  32.2 0.1 eq.25
  32.3 0.6 reduce-window.6
  32.9 0.2 slice_reduce_fusion
  33.2 0.1 copy.17
  33.3 0.1 mul.509
  33.5 0.1 fusion.42
  33.6 1.4 scatter_custom_fusion
  35.0 28.6 %reduce-scatter.3.cloned.1.call-done = bf16[128,2048]{1,0:T(8,128)(2,1)} async-done(((bf16[512,2048]{1,0:T(8,128)(2,1)}), bf16[128,2048]{1,0:T(8,128)(2,1)}) %reduce-scatter.3.cloned.1.call-update) | async-done | bytes 524304 | tf_op jit(solution)/shard_map/reduce_scatter | solution.py:81
  63.6 0.0 copy-done.1
  63.6 0.0 copy-start.2
  63.6 1.3 fusion.35
  65.0 1.3 multiply_reduce_fusion.1
  66.3 0.0 copy-done.3
  66.3 0.0 copy-done.2
  66.3 0.3 multiply_convert_fusion.2
  66.7 3.3 gather_fusion
  70.0 53.7 %all_to_all.10 = bf16[8,64,2048]{2,1,0:T(8,128)(2,1)} all-to-all(bf16[8,64,2048]{2,1,0:T(8,128)(2,1)} %bitcast.69), channel_id=1, replica_groups=mesh['sp'=8,'tp'=4] {'sp'}, dimensions={0} | all-to-all | bytes 4194304 | tf_op jit(solution)/shard_map/all_to_all | solution.py:98
  123.7 0.0 all-gather.3.cloned.1.call-update
  123.7 0.2 reduce-scatter.5.cloned.1.call-start
  124.0 56.3 %all-gather.3.cloned.1.call-done = bf16[32,64,2048]{2,1,0:T(8,128)(2,1)} async-done(((bf16[8,64,2048]{2,1,0:T(8,128)(2,1)}), bf16[32,64,2048]{2,1,0:T(8,128)(2,1)}) %all-gather.3.cloned.1.call-update) | async-done | bytes 8388624 | tf_op jit(solution)/shard_map/all_gather | solution.py:99
  180.2 0.0 copy-start.7
  180.2 0.0 copy-start.8
  180.2 7.7 %fusion.2 = f32[2048,512]{1,0:T(8,128)S(1)} fusion(bf16[2048,2048]{1,0:T(8,128)(2,1)} %bitcast.106, bf16[1,2048,512]{2,1,0:T(8,128)(2,1)} %param.23), kind=kOutput, calls=%fused_computation.8 | convolution fusion | flops 4294967296 | bytes 14680064 | tf_op jit(solution)/shard_map/dot_general | solution.py:40
  187.9 0.0 copy-done.7
  187.9 0.0 copy-done.8
  187.9 5.7 %multiply_convert_fusion = bf16[2048,512]{1,0:T(8,128)(2,1)S(1)} fusion(f32[2048,512]{1,0:T(8,128)S(1)} %fusion.2, bf16[2048,2048]{1,0:T(8,128)(2,1)S(1)} %bitcast.107, bf16[1,2048,512]{2,1,0:T(8,128)(2,1)S(1)} %copy-done.8), kind=kOutput, calls=%fused_computation.4 | convolution fusion | flops 4305453056 | bytes 16777216 | tf_op jit(solution)/shard_map/dot_general | solution.py:39
  193.6 0.0 copy-done
  193.7 6.8 %convolution_convert_fusion = bf16[2048,2048]{1,0:T(8,128)(2,1)} fusion(bf16[2048,512]{1,0:T(8,128)(2,1)S(1)} %multiply_convert_fusion, bf16[1,512,2048]{2,1,0:T(8,128)(2,1)S(1)} %copy-done), kind=kOutput, calls=%fused_computation.3 | convolution fusion | flops 4299161600 | bytes 12582912 | tf_op jit(solution)/shard_map/dot_general | solution.py:107
  200.4 0.0 reduce-scatter.5.cloned.1.call-update
  200.5 71.5 %reduce-scatter.5.cloned.1.call-done = bf16[512,2048]{1,0:T(8,128)(2,1)} async-done(((bf16[2048,2048]{1,0:T(8,128)(2,1)}), bf16[512,2048]{1,0:T(8,128)(2,1)}) %reduce-scatter.5.cloned.1.call-update) | async-done | bytes 2097168 | tf_op jit(solution)/shard_map/reduce_scatter | solution.py:106
  272.0 0.0 copy-start.6
  272.0 5.6 %all-to-all-start.1 = ((bf16[8,64,2048]{2,1,0:T(8,128)(2,1)}), bf16[8,64,2048]{2,1,0:T(8,128)(2,1)}, u32[]{:S(2)}, u32[]{:S(2)}) async-start(bf16[8,64,2048]{2,1,0:T(8,128)(2,1)} %bitcast.70), calls=%async_computation.3 | async-start | bytes 4194304 | tf_op jit(solution)/shard_map/all_to_all | solution.py:113
  277.7 0.0 copy-done.6
  277.7 0.2 copy.20
  277.9 48.0 %all-to-all-done.1 = bf16[8,64,2048]{2,1,0:T(8,128)(2,1)} async-done(((bf16[8,64,2048]{2,1,0:T(8,128)(2,1)}), bf16[8,64,2048]{2,1,0:T(8,128)(2,1)}, u32[]{:S(2)}, u32[]{:S(2)}) %all-to-all-start.1) | async-done | bytes 2097184 | tf_op jit(solution)/shard_map/all_to_all | solution.py:113
  325.9 5.2 %gather_fusion.1 = bf16[256,2048]{1,0:T(8,128)(2,1)} fusion(bf16[512,2048]{1,0:T(8,128)(2,1)} %bitcast.41, s32[1024]{0:T(1024)S(1)} %pad_clamp_fusion), kind=kCustom, calls=%fused_computation.1 | custom fusion | bytes 2098176 | tf_op jit(solution)/shard_map/gather | solution.py:114
  331.1 2.5 reshape.97
  333.6 2.5 fusion.51
  336.1 0.0 copy-start.4
  336.1 0.6 fusion.40
  336.7 0.4 multiply_reduce_fusion
  337.1 0.0 copy-done.4
  337.1 1.3 multiply_convert_fusion.1
  (16 shorter events, 0.2 us)
Async XLA Ops:
  6.5 187.1 %copy-start = (bf16[1,512,2048]{2,1,0:T(8,128)(2,1)S(1)}, bf16[1,512,2048]{2,1,0:T(8,128)(2,1)}, u32[]{:S(2)}) copy-start(bf16[1,512,2048]{2,1,0:T(8,128)(2,1)} %param.24) | copy-start | bytes 6291460
  6.5 57.1 %reduce-scatter.3.cloned.1.call-start = ((), (), s32[]{:S(2)}) async-start(), calls=%async_computation.4 | async-start | bytes 2621440 | tf_op jit(solution)/shard_map/reduce_scatter | solution.py:81
  8.2 7.1 %collective-permute-start = (bf16[30,512]{1,0:T(8,128)(2,1)S(1)}, bf16[30,512]{1,0:T(8,128)(2,1)S(1)}, u32[]{:S(2)}, u32[]{:S(2)}) collective-permute-start(bf16[30,512]{1,0:T(8,128)(2,1)S(1)} %slice.264), channel_id=1, source_target_pairs={{0,4},{4,8},{8,12},{12,16},{16,20},{20,24},{24,28},{1,5},{5,9},{9,... | collective-permute-start | bytes 92168 | tf_op jit(solution)/shard_map/ppermute | solution.py:17
  15.5 11.4 %copy-start.9 = (f32[512]{0:T(512)S(1)}, f32[512]{0:T(512)}, u32[]{:S(2)}) copy-start(f32[512]{0:T(512)} %param.16) | copy-start | bytes 6148
  31.3 0.7 copy-start.5
  31.3 32.4 %copy-start.1 = (bf16[128,2048]{1,0:T(8,128)(2,1)S(1)}, bf16[128,2048]{1,0:T(8,128)(2,1)}, u32[]{:S(2)}) copy-start(bf16[128,2048]{1,0:T(8,128)(2,1)} %param.18) | copy-start | bytes 1572868
  31.3 35.1 %copy-start.3 = (f32[2048]{0:T(1024)S(1)}, f32[2048]{0:T(1024)}, u32[]{:S(2)}) copy-start(f32[2048]{0:T(1024)} %param.19) | copy-start | bytes 24580
  31.3 148.9 %all-gather.3.cloned.1.call-start = ((), (), s32[]{:S(2)}) async-start(), calls=%async_computation.6 | async-start | bytes 10485760 | tf_op jit(solution)/shard_map/all_gather | solution.py:99
  63.6 2.7 copy-start.2
  123.7 148.3 %reduce-scatter.5.cloned.1.call-start = ((), (), s32[]{:S(2)}) async-start(), calls=%async_computation.5 | async-start | bytes 10485760 | tf_op jit(solution)/shard_map/reduce_scatter | solution.py:106
  180.2 7.7 %copy-start.7 = (bf16[32,64,2048]{2,1,0:T(8,128)(2,1)S(1)}, bf16[32,64,2048]{2,1,0:T(8,128)(2,1)}, u32[]{:S(2)}) copy-start(bf16[32,64,2048]{2,1,0:T(8,128)(2,1)} %all-gather.3.cloned.1.call-done) | copy-start | bytes 25165828
  180.2 7.7 %copy-start.8 = (bf16[1,2048,512]{2,1,0:T(8,128)(2,1)S(1)}, bf16[1,2048,512]{2,1,0:T(8,128)(2,1)}, u32[]{:S(2)}) copy-start(bf16[1,2048,512]{2,1,0:T(8,128)(2,1)} %param.22) | copy-start | bytes 6291460
  272.0 5.7 %copy-start.6 = (f32[128,2]{0,1:T(2,128)S(1)}, f32[128,2]{0,1:T(2,128)}, u32[]{:S(2)}) copy-start(f32[128,2]{0,1:T(2,128)} %param.21) | copy-start | bytes 3076
  272.0 53.8 %all-to-all-start.1 = ((bf16[8,64,2048]{2,1,0:T(8,128)(2,1)}), bf16[8,64,2048]{2,1,0:T(8,128)(2,1)}, u32[]{:S(2)}, u32[]{:S(2)}) async-start(bf16[8,64,2048]{2,1,0:T(8,128)(2,1)} %bitcast.70), calls=%async_computation.3 | async-start | bytes 4194304 | tf_op jit(solution)/shard_map/all_to_all | solution.py:113
  336.1 1.0 copy-start.4
Sparse Core Ops, SparseCore 0:
  31.4 32.1 reduce-scatter.2
  123.8 56.3 all-gather.2
  200.6 71.3 reduce-scatter.4
where the time goes:
time: 346 us; the launch traced here: 345 us
  waiting for transfers between devices  205 us (59%)
  blocking collectives  60 us (17%)
  matrix products  27 us (8%)
  local copies, waits for them, and re-layouts  16.4 us (5%)
  between operations  13.3 us (4%)
  other arithmetic  12.9 us (4%)
  starting transfers between devices  10.8 us (3%)
    reduce_scatter x1, waiting for transfers between devices, shards(): lax.psum_scatter(jnp.dot(section, down_local, preferred_element_type=jnp....  71.5 us
    all_gather x1, waiting for transfers between devices, shards(): activate_arrived = lax.all_gather(arrived[None], 'tp', axis=0, tiled=True)  56.3 us
    all_to_all x1, blocking collectives, shards(): lax.all_to_all(dispatched, 'sp', split_axis=0, concat_axis=0, tiled=True)  53.7 us
    all_to_all x1, waiting for transfers between devices, shards(): lax.all_to_all(expert_out, 'sp', split_axis=0, concat_axis=0, tiled=True)  48 us
    reduce_scatter x1, waiting for transfers between devices, shards(): lax.psum_scatter(jnp.dot(section, mix_weight, preferred_element_type=jnp....  28.6 us
    dot_general x1, matrix products, expert_activity(): up_pre = jnp.dot(tokens, up_matrix, preferred_element_type=jnp.float32)  7.67 us
  transfers between devices with their start and end apart: 5, of which 4 were waited for; matrix products, arithmetic and copies ran while one was open for 2% of the time, Pallas kernels for 0%

commit v1 on v0

v1 whole, which is shorter than its diff:
```python
import functools

import jax
import jax.numpy as jnp
from jax import lax
from jax.experimental import pallas as pl
from jax.experimental.pallas import tpu as pltpu
from jax.sharding import PartitionSpec as P


DC = 2048


EPSILON = 1e-05
LIMIT = 7.0
SLOPE = 1.702


def shifted(block, axis, distance):
    devices = range(lax.axis_size(axis))
    route = [(i - distance, i) for i in devices if i - distance in devices]
    return lax.ppermute(block, axis, route)


def normalize(values, gain_vector):
    centre = jnp.mean(values, axis=-1, keepdims=True)
    spread = jnp.mean(jnp.square(values - centre), axis=-1, keepdims=True)
    return (values - centre) * lax.rsqrt(spread + EPSILON) * gain_vector


def swapped(block, stride):
    route = [(i, i ^ stride) for i in range(lax.axis_size("tp"))]
    return lax.ppermute(block, "tp", route)


def slot_layout(route_ids, experts, capacity):
    row_count, top_count = route_ids.shape
    flat_ids = route_ids.reshape(row_count * top_count)
    onehot = (flat_ids[:, None] == jnp.arange(experts, dtype=jnp.int32)[None, :]).astype(jnp.int32)
    before = jnp.cumsum(onehot, axis=0) - onehot
    slot_rank = jnp.sum(before * onehot, axis=1)
    position = flat_ids * capacity + slot_rank
    return position.reshape(row_count, top_count)


def expert_activity(tokens, gate_matrix, up_matrix):
    gate_pre = jnp.dot(tokens, gate_matrix, preferred_element_type=jnp.float32)
    up_pre = jnp.dot(tokens, up_matrix, preferred_element_type=jnp.float32)
    gated = jnp.minimum(gate_pre, LIMIT)
    upper = jnp.clip(up_pre, -LIMIT, LIMIT)
    return ((upper + 1.0) * gated * jax.nn.sigmoid(SLOPE * gated)).astype(jnp.bfloat16)


MESH = pl.DeviceIdType.MESH


def exchange_kernel(count, forward, sent, out, local_sem, send_sem, recv_sem, pass_sem, land_sem):
    me = lax.axis_index("sp")
    place = lax.axis_index("tp")
    partner = place + 1 - 2 * lax.rem(place, 2)
    mine = out.at[0] if forward else out

    barrier = pltpu.get_barrier_semaphore()
    for step in range(1, count):
        peer = lax.rem(me + step, count)
        pl.semaphore_signal(barrier, inc=1, device_id={"sp": peer}, device_id_type=MESH)
    if forward:
        pl.semaphore_signal(barrier, inc=1, device_id={"tp": partner}, device_id_type=MESH)
    pl.semaphore_wait(barrier, count - 1 + int(forward))

    copies = []
    for step in range(1, count):
        peer = lax.rem(me + step, count)
        copy = pltpu.make_async_remote_copy(
            src_ref=sent.at[peer],
            dst_ref=mine.at[me],
            send_sem=send_sem.at[step],
            recv_sem=recv_sem.at[step],
            device_id={"sp": peer},
            device_id_type=MESH,
        )
        copy.start()
        copies.append(copy)
    kept = pltpu.make_async_copy(sent.at[me], mine.at[me], local_sem)
    kept.start()

    def passed(block, source, step):
        return pltpu.make_async_remote_copy(
            src_ref=block,
            dst_ref=out.at[1, source],
            send_sem=pass_sem.at[step],
            recv_sem=land_sem.at[step],
            device_id={"tp": partner},
            device_id_type=MESH,
        )

    passes = []
    if forward:
        passes.append(passed(sent.at[me], me, 0))
        passes[0].start()
    order = sorted(range(1, count), key=lambda step: min(step, count - step))
    for step in order:
        source = lax.rem(me + count - step, count)
        pltpu.make_async_remote_copy(
            src_ref=sent.at[source],
            dst_ref=mine.at[source],
            send_sem=send_sem.at[step],
            recv_sem=recv_sem.at[step],
            device_id={"sp": source},
            device_id_type=MESH,
        ).wait_recv()
        if forward:
            one = passed(mine.at[source], source, step)
            one.start()
            passes.append(one)
    kept.wait()
    for copy in copies:
        copy.wait_send()
    for one in passes:
        one.wait()


def exchange(blocks, forward, number):
    count = blocks.shape[0]
    shape = ((2,) if forward else ()) + blocks.shape
    size = blocks.size * 2
    return pl.pallas_call(
        functools.partial(exchange_kernel, count, forward),
        out_shape=jax.ShapeDtypeStruct(shape, blocks.dtype),
        in_specs=[pl.BlockSpec(memory_space=pl.ANY)],
        out_specs=pl.BlockSpec(memory_space=pl.ANY),
        scratch_shapes=[
            pltpu.SemaphoreType.DMA,
            pltpu.SemaphoreType.DMA((count,)),
            pltpu.SemaphoreType.DMA((count,)),
            pltpu.SemaphoreType.DMA((count,)),
            pltpu.SemaphoreType.DMA((count,)),
        ],
        compiler_params=pltpu.CompilerParams(collective_id=number, has_side_effects=True),
        cost_estimate=pl.CostEstimate(flops=0, bytes_accessed=size * 40, transcendentals=0),
    )(blocks)


def shards(
    glu_value,
    glu_gate,
    conv_kernel,
    norm_gain,
    mix_weight,
    residual,
    resid_gain,
    expert_ids,
    route_weight,
    w_gate,
    w_up,
    w_down,
    out_gain,
):
    gate_local, up_local, down_local = w_gate[0], w_up[0], w_down[0]
    depth = gate_local.shape[0]
    first, second = depth // 2, depth * 3 // 4
    left = down_local.shape[1] * 3 // 8
    gate_far = jnp.concatenate(
        [
            swapped(gate_local[:first], 2),
            swapped(gate_local[first:second], 2),
            swapped(gate_local[second:], 2),
        ],
        axis=0,
    )
    up_far = swapped(up_local, 2)
    down_far = (swapped(down_local[:, :left], 2), swapped(down_local[:, left:], 2))
    gated_in = (
        glu_value.astype(jnp.float32) * jax.nn.sigmoid(glu_gate.astype(jnp.float32))
    ).astype(jnp.bfloat16)
    reach_back = conv_kernel.shape[0] - 1
    length = gated_in.shape[0]
    before_rows = shifted(gated_in[length - reach_back :], "sp", 1)
    extended = jnp.concatenate([before_rows, gated_in], axis=0).astype(jnp.float32)
    convolved = jnp.zeros(gated_in.shape, jnp.float32)
    for offset in range(reach_back + 1):
        convolved = convolved + conv_kernel[offset] * extended[offset : offset + length]
    channel_sum, squares = lax.psum(
        (jnp.sum(convolved, axis=1), jnp.sum(convolved * convolved, axis=1)), "tp"
    )
    centre = channel_sum / DC
    spread = squares / DC - centre * centre
    normed = (convolved - centre[:, None]) * lax.rsqrt(spread[:, None] + EPSILON) * norm_gain
    mix_in = jax.nn.silu(normed).astype(jnp.bfloat16)
    tp_count = lax.axis_size("tp")
    place = lax.axis_index("tp")
    own_count = length // tp_count
    width = residual.shape[1]
    products = jnp.dot(mix_in, mix_weight, preferred_element_type=jnp.float32)
    products = products.astype(jnp.bfloat16).reshape(tp_count // 2, 2, own_count, width)
    near = place % 2
    far = place // 2
    kept = lax.dynamic_index_in_dim(products, near, 1, False)
    given = lax.dynamic_index_in_dim(products, 1 - near, 1, False)
    pair_sum = kept.astype(jnp.float32) + swapped(given, 1).astype(jnp.float32)
    pair_kept = lax.dynamic_index_in_dim(pair_sum, far, 0, False)
    pair_given = lax.dynamic_index_in_dim(pair_sum, 1 - far, 0, False).astype(jnp.bfloat16)
    mixed_rows = pair_kept + swapped(pair_given, 2).astype(jnp.float32)
    hidden = normalize(residual.astype(jnp.float32) + mixed_rows, resid_gain).astype(jnp.bfloat16)
    experts = lax.axis_size("sp")
    top_count = expert_ids.shape[1]
    capacity = 2 * own_count * top_count // experts
    positions = slot_layout(expert_ids, experts, capacity)
    slots = jnp.arange(experts * capacity, dtype=jnp.int32)
    chosen = (positions[:, :, None] == slots).astype(jnp.float32)
    pick = jnp.sum(chosen, axis=1).astype(jnp.bfloat16)
    weights = jnp.sum(chosen * route_weight[:, :, None], axis=1)
    weights_high = weights.astype(jnp.bfloat16)
    weights_low = (weights - weights_high.astype(jnp.float32)).astype(jnp.bfloat16)
    dispatched = lax.dot_general(
        pick, hidden, (((0,), (0,)), ((), ())), preferred_element_type=jnp.float32
    ).astype(jnp.bfloat16)
    dispatched = dispatched.reshape(experts, capacity, width)
    arrived = exchange(dispatched, True, 0)
    rows = arrived.reshape(2 * experts * capacity, width)
    act_local = expert_activity(rows, gate_local, up_local)
    act_far = expert_activity(rows, gate_far, up_far)
    sums = []
    for part in range(2):
        columns = slice(0, left) if part == 0 else slice(left, width)
        share = down_far[part].shape[1]
        out = jnp.dot(
            act_local, down_local[:, columns], preferred_element_type=jnp.float32
        ) + jnp.dot(act_far, down_far[part], preferred_element_type=jnp.float32)
        out = out.astype(jnp.bfloat16).reshape(2, experts * capacity, share)
        given_out = swapped(out[1], 1)
        expert_out = (out[0].astype(jnp.float32) + given_out.astype(jnp.float32)).astype(jnp.bfloat16)
        returned = exchange(expert_out.reshape(experts, capacity, share), False, 1 + part)
        returned = returned.reshape(experts * capacity, share)
        sums.append(
            jnp.dot(weights_high, returned, preferred_element_type=jnp.float32)
            + jnp.dot(weights_low, returned, preferred_element_type=jnp.float32)
        )
    routed_sum = jnp.concatenate(sums, axis=1)
    return normalize(hidden.astype(jnp.float32) + routed_sum, out_gain).astype(jnp.bfloat16)


def solution(mesh):
    in_specs = (
        P("sp", "tp"),
        P("sp", "tp"),
        P(None, "tp"),
        P("tp"),
        P("tp", None),
        P(("sp", "tp"), None),
        P(),
        P(("sp", "tp"), None),
        P(("sp", "tp"), None),
        P("sp", None, "tp"),
        P("sp", None, "tp"),
        P("sp", "tp", None),
        P(),
    )
    out_specs = P(("sp", "tp"), None)

    return jax.shard_map(shards, mesh=mesh, in_specs=in_specs, out_specs=out_specs, check_vma=False)
```

time: 346 us -> 295 us (0.85)
  the two profiles are of different devices: /device:TPU:0 before, /device:TPU:12 now
where the time goes in v1:
time: 295 us
  waiting for transfers between devices  111 us (38%)
  Pallas kernels  107 us (36%)
  matrix products  31.5 us (11%)
  other arithmetic  17.4 us (6%)
  local copies, waits for them, and re-layouts  11 us (4%)
  starting transfers between devices  10.6 us (4%)
  blocking collectives  6.15 us (2%)
    ppermute x10, waiting for transfers between devices, swapped(): return lax.ppermute(block, 'tp', route)  111 us
    pallas_call x3, Pallas kernels, exchange(): pl.pallas_call(functools.partial(exchange_kernel, count, forward), out_sh...  107 us
    dot_general x2, matrix products, expert_activity(): up_pre = jnp.dot(tokens, up_matrix, preferred_element_type=jnp.float32)  9.23 us
    dot_general x2, matrix products, expert_activity(): gate_pre = jnp.dot(tokens, gate_matrix, preferred_element_type=jnp.float32)  7.22 us
    ppermute x10, starting transfers between devices, swapped(): return lax.ppermute(block, 'tp', route)  7.17 us
    psum x1, blocking collectives, shards(): lax.psum((jnp.sum(convolved, axis=1), jnp.sum(convolved * convolved, axis...  6.15 us
  transfers between devices with their start and end apart: 11, of which 3 were waited for; matrix products, arithmetic and copies ran while one was open for 14% of the time, Pallas kernels for 25%

profile of v1, /device:TPU:12, one launch (start us, length us, event | category | flops | bytes accessed | tf_op | source)
XLA Modules:
  0.0 294.6 jit_solution(8578751106224354302)
XLA Ops:
  0.0 1.6 multiply_convert_fusion.5
  1.7 3.4 %collective-permute-start = (bf16[30,512]{1,0:T(8,128)(2,1)S(1)}, bf16[30,512]{1,0:T(8,128)(2,1)S(1)}, u32[]{:S(2)}, u32[]{:S(2)}) collective-permute-start(bf16[30,512]{1,0:T(8,128)(2,1)S(1)} %slice.314), channel_id=1, source_target_pairs={{0,4},{4,8},{8,12},{12,16},{16,20},{20,24},{24,28},{1,5},{5,9},{9,... | collective-permute-start | bytes 92168 | tf_op jit(solution)/shard_map/ppermute | solution.py:22
  5.1 1.2 fusion.69
  6.3 1.0 fusion.70
  7.3 0.2 collective-permute-done
  7.5 0.2 maximum_convert_fusion
  7.6 0.0 copy-start.18
  7.7 5.1 %fusion.65 = (f32[512]{0:T(512)S(1)}, f32[512]{0:T(512)S(1)}, f32[512,512]{1,0:T(8,128)S(1)}) fusion(f32[542,512]{1,0:T(8,128)S(1)} %maximum_convert_fusion, f32[512]{0:T(512)S(1)} %bitcast.139, f32[512]{0:T(512)S(1)} %bitcast.140, f32[512]{0:T(512)S(1)} %bitcast.111, f32[512]{0:T(512)S(1)} %bitcast.112, f32[512]{0:T(512)S(1)} %bitcast.113, ...), kind=kLoop, calls=%fused_computation.133 | loop fusion | flops 16776192 | bytes 33622016 | tf_op jit(solution)/shard_map/reduce_sum | solution.py:184
  12.7 6.1 %all-reduce = (f32[512]{0:T(512)S(1)}, f32[512]{0:T(512)S(1)}) all-reduce(f32[512]{0:T(512)S(1)} %get-tuple-element.6, f32[512]{0:T(512)S(1)} %get-tuple-element.5), channel_id=1, replica_groups=mesh['sp'=8,'tp'=4] {'tp'}, use_global_device_ids=true, to_apply=%region_3.0 | all-reduce | flops 1024 | bytes 8192 | tf_op jit(solution)/shard_map/psum | solution.py:183
  18.9 1.4 convolution_convert_fusion.1
  20.4 1.1 dynamic-slice_bitcast_fusion
  21.4 1.2 collective-permute-start.3
  22.7 0.4 copy-done.10
  23.1 1.0 slice_bitcast_fusion.2
  24.1 1.2 collective-permute-start.5
  25.4 0.8 collective-permute-start.6
  26.1 1.0 slice_bitcast_fusion
  27.2 1.2 collective-permute-start.4
  28.4 0.1 copy.30
  28.6 0.1 eq.44
  28.7 0.1 eq.40
  28.9 1.0 slice.347
  29.8 1.3 slice.350
  31.1 0.7 reduce-window.6
  31.9 1.6 convert_add_fusion
  33.5 0.1 fusion.43
  33.5 0.8 collective-permute-start.2
  34.4 0.2 slice_reduce_fusion
  34.6 0.1 fusion.51
  34.7 0.1 reduce_sum.88
  34.9 0.1 copy.32
  34.9 0.0 copy-done.17
  35.0 0.2 select_reduce_fusion
  35.1 90.7 %collective-permute-done.2 = bf16[128,2048]{1,0:T(8,128)(2,1)S(1)} collective-permute-done((bf16[128,2048]{1,0:T(8,128)(2,1)S(1)}, bf16[128,2048]{1,0:T(8,128)(2,1)S(1)}, u32[]{:S(2)}, u32[]{:S(2)}) %collective-permute-start.2) | collective-permute-done | bytes 524320 | tf_op jit(solution)/shard_map/ppermute | solution.py:33
  125.9 0.8 copy-done.13
  126.7 1.2 collective-permute-start.7
  127.9 1.8 fusion.66
  129.7 0.3 multiply_reduce_fusion.1
  130.0 2.1 convolution_convert_fusion
  132.2 53.0 %shard_map.127 = bf16[2,8,64,2048]{3,2,1,0:T(8,128)(2,1)} custom-call(bf16[8,64,2048]{2,1,0:T(8,128)(2,1)} %bitcast.95), custom_call_target="tpu_custom_call" | custom-call | bytes 83886080 | tf_op jit(solution)/shard_map/pallas_call | solution.py:127
  185.2 5.3 %fusion.54 = f32[1024,512]{1,0:T(8,128)S(1)} fusion(bf16[1024,2048]{1,0:T(8,128)(2,1)} %bitcast.99, bf16[1,2048,512]{2,1,0:T(8,128)(2,1)} %param.23), kind=kOutput, calls=%fused_computation.122 | convolution fusion | flops 2147483648 | bytes 8388608 | tf_op jit(solution)/shard_map/dot_general | solution.py:48
  190.5 2.8 multiply_convert_fusion.1
  193.4 1.0 fusion.61
  194.4 1.5 fusion.63
  195.9 0.4 collective-permute-start.9
  196.3 3.9 %fusion.71 = f32[1024,512]{1,0:T(8,128)S(1)} fusion(bf16[1024,2048]{1,0:T(8,128)(2,1)S(1)} %bitcast.101, bf16[2048,512]{1,0:T(8,128)(2,1)} %collective-permute-done.3), kind=kOutput, calls=%fused_computation.137 | convolution fusion | flops 2147483648 | bytes 8388608 | tf_op jit(solution)/shard_map/dot_general | solution.py:48
  200.2 4.4 %multiply_convert_fusion = bf16[1024,512]{1,0:T(8,128)(2,1)S(1)} fusion(f32[1024,512]{1,0:T(8,128)S(1)} %fusion.71, bf16[1024,2048]{1,0:T(8,128)(2,1)S(1)} %bitcast.102, bf16[512,512]{1,0:T(8,128)(2,1)} %collective-permute-done.6, bf16[512,512]{1,0:T(8,128)(2,1)} %collective-permute-done.5, bf16[1024,512]{1,0:T(8,128)(2,1)} %collective-permute-done.4), kind=kOutput, calls=%fused_computation.15 | convolution fusion | flops 2159017984 | bytes 9437184 | tf_op jit(solution)/shard_map/dot_general | solution.py:47
  204.6 2.4 add_convert_fusion.1
  207.0 0.1 slice.349
  207.1 0.2 collective-permute-start.8
  207.2 19.8 %collective-permute-done.9 = bf16[512,1280]{1,0:T(8,128)(2,1)S(1)} collective-permute-done((bf16[512,1280]{1,0:T(8,128)(2,1)S(1)}, bf16[512,1280]{1,0:T(8,128)(2,1)S(1)}, u32[]{:S(2)}, u32[]{:S(2)}) %collective-permute-start.9) | collective-permute-done | bytes 1310752 | tf_op jit(solution)/shard_map/ppermute | solution.py:33
  227.1 1.5 add_convert_fusion
  228.6 1.3 slice.352
  229.9 1.1 add_convert_fusion.3
  231.0 21.5 %shard_map.128 = bf16[8,64,768]{2,1,0:T(8,128)(2,1)} custom-call(bf16[8,64,768]{2,1,0:T(8,128)(2,1)} %bitcast.107), custom_call_target="tpu_custom_call" | custom-call | bytes 31457280 | tf_op jit(solution)/shard_map/pallas_call | solution.py:127
  252.5 1.6 fusion.59
  254.1 1.4 convolution_add_fusion.1
  255.5 2.7 add_convert_fusion.2
  258.2 32.1 %shard_map.129 = bf16[8,64,1280]{2,1,0:T(8,128)(2,1)} custom-call(bf16[8,64,1280]{2,1,0:T(8,128)(2,1)} %bitcast.98), custom_call_target="tpu_custom_call" | custom-call | bytes 52428800 | tf_op jit(solution)/shard_map/pallas_call | solution.py:127
  290.4 1.8 fusion.58
  292.1 0.3 convolution_add_fusion
  292.5 0.3 fusion.49
  292.9 0.4 multiply_reduce_fusion
  293.3 1.3 multiply_convert_fusion.2
  (54 shorter events, 0.2 us)
Async XLA Ops:
  0.0 18.9 %copy-start = (bf16[512,2048]{1,0:T(8,128)(2,1)S(1)}, bf16[512,2048]{1,0:T(8,128)(2,1)}, u32[]{:S(2)}) copy-start(bf16[512,2048]{1,0:T(8,128)(2,1)} %param.17) | copy-start | bytes 6291460
  1.7 5.8 %collective-permute-start = (bf16[30,512]{1,0:T(8,128)(2,1)S(1)}, bf16[30,512]{1,0:T(8,128)(2,1)S(1)}, u32[]{:S(2)}, u32[]{:S(2)}) collective-permute-start(bf16[30,512]{1,0:T(8,128)(2,1)S(1)} %slice.314), channel_id=1, source_target_pairs={{0,4},{4,8},{8,12},{12,16},{16,20},{20,24},{24,28},{1,5},{5,9},{9,... | collective-permute-start | bytes 92168 | tf_op jit(solution)/shard_map/ppermute | solution.py:22
  7.6 11.2 %copy-start.18 = (f32[512]{0:T(512)S(1)}, f32[512]{0:T(512)}, u32[]{:S(2)}) copy-start(f32[512]{0:T(512)} %param.16) | copy-start | bytes 6148
  20.3 3.8 %copy-start.9 = (bf16[512,2048]{1,0:T(8,128)(2,1)}, bf16[512,2048]{1,0:T(8,128)(2,1)S(1)}, u32[]{:S(2)}) copy-start(bf16[512,2048]{1,0:T(8,128)(2,1)S(1)} %convolution_convert_fusion.1) | copy-start | bytes 6291460
  20.4 2.7 copy-start.10
  21.4 10.4 %collective-permute-start.1 = (bf16[2,128,2048]{2,1,0:T(8,128)(2,1)}, bf16[2,128,2048]{2,1,0:T(8,128)(2,1)S(1)}, u32[]{:S(2)}, u32[]{:S(2)}) collective-permute-start(bf16[2,128,2048]{2,1,0:T(8,128)(2,1)} %dynamic-slice_bitcast_fusion), channel_id=1, source_target_pairs={{0,1},{1,0},{2,3},{3,2},{4,5},{5,4},{6,7},{7,6},{8,9},{9,8},{10,11... | collective-permute-start | bytes 3145736 | tf_op jit(solution)/shard_map/ppermute | solution.py:33
  21.4 7.0 %copy-start.16 = (s32[128,2]{0,1:T(2,128)S(1)}, s32[128,2]{0,1:T(2,128)}, u32[]{:S(2)}) copy-start(s32[128,2]{0,1:T(2,128)} %param.20) | copy-start | bytes 3076
  21.4 7.4 %copy-start.7 = (bf16[1,512,2048]{2,1,0:T(8,128)(2,1)S(1)}, bf16[1,512,2048]{2,1,0:T(8,128)(2,1)}, u32[]{:S(2)}) copy-start(bf16[1,512,2048]{2,1,0:T(8,128)(2,1)} %param.24) | copy-start | bytes 6291460
  21.4 174.5 %collective-permute-start.3 = (bf16[2048,512]{1,0:T(8,128)(2,1)}, bf16[2048,512]{1,0:T(8,128)(2,1)}, u32[]{:S(2)}, u32[]{:S(2)}) collective-permute-start(bf16[2048,512]{1,0:T(8,128)(2,1)} %bitcast.40), channel_id=1, source_target_pairs={{0,2},{1,3},{2,0},{3,1},{4,6},{5,7},{6,4},{7,5},{8,10},{9,11},{10,... | collective-permute-start | bytes 6291464 | tf_op jit(solution)/shard_map/ppermute | solution.py:33
  24.1 176.1 %collective-permute-start.5 = (bf16[512,512]{1,0:T(8,128)(2,1)}, bf16[512,512]{1,0:T(8,128)(2,1)}, u32[]{:S(2)}, u32[]{:S(2)}) collective-permute-start(bf16[512,512]{1,0:T(8,128)(2,1)} %get-tuple-element.14), channel_id=1, source_target_pairs={{0,2},{1,3},{2,0},{3,1},{4,6},{5,7},{6,4},{7,5},{8,10},{9,11},{10,... | collective-permute-start | bytes 1572872 | tf_op jit(solution)/shard_map/ppermute | solution.py:33
  25.4 174.9 %collective-permute-start.6 = (bf16[512,512]{1,0:T(8,128)(2,1)}, bf16[512,512]{1,0:T(8,128)(2,1)}, u32[]{:S(2)}, u32[]{:S(2)}) collective-permute-start(bf16[512,512]{1,0:T(8,128)(2,1)} %get-tuple-element.15), channel_id=1, source_target_pairs={{0,2},{1,3},{2,0},{3,1},{4,6},{5,7},{6,4},{7,5},{8,10},{9,11},{10,... | collective-permute-start | bytes 1572872 | tf_op jit(solution)/shard_map/ppermute | solution.py:33
  27.2 173.0 %collective-permute-start.4 = (bf16[1024,512]{1,0:T(8,128)(2,1)}, bf16[1024,512]{1,0:T(8,128)(2,1)}, u32[]{:S(2)}, u32[]{:S(2)}) collective-permute-start(bf16[1024,512]{1,0:T(8,128)(2,1)} %slice_bitcast_fusion), channel_id=1, source_target_pairs={{0,2},{1,3},{2,0},{3,1},{4,6},{5,7},{6,4},{7,5},{8,10},{9,11},{10,... | collective-permute-start | bytes 3145736 | tf_op jit(solution)/shard_map/ppermute | solution.py:33
  31.8 3.1 %copy-start.17 = (f32[128,2]{0,1:T(2,128)S(1)}, f32[128,2]{0,1:T(2,128)}, u32[]{:S(2)}) copy-start(f32[128,2]{0,1:T(2,128)} %param.21) | copy-start | bytes 3076
  33.4 1.5 copy-start.5
  33.5 92.3 %collective-permute-start.2 = (bf16[128,2048]{1,0:T(8,128)(2,1)S(1)}, bf16[128,2048]{1,0:T(8,128)(2,1)S(1)}, u32[]{:S(2)}, u32[]{:S(2)}) collective-permute-start(bf16[128,2048]{1,0:T(8,128)(2,1)S(1)} %fusion.43), channel_id=1, source_target_pairs={{0,2},{1,3},{2,0},{3,1},{4,6},{5,7},{6,4},{7,5},{8,10},{9,11},{10,... | collective-permute-start | bytes 1572872 | tf_op jit(solution)/shard_map/ppermute | solution.py:33
  35.1 94.9 %copy-start.14 = (f32[2048]{0:T(1024)S(1)}, f32[2048]{0:T(1024)}, u32[]{:S(2)}) copy-start(f32[2048]{0:T(1024)} %param.19) | copy-start | bytes 24580
  125.9 0.8 copy-start.13
  126.7 78.0 %collective-permute-start.7 = (bf16[512,768]{1,0:T(8,128)(2,1)}, bf16[512,768]{1,0:T(8,128)(2,1)}, u32[]{:S(2)}, u32[]{:S(2)}) collective-permute-start(bf16[512,768]{1,0:T(8,128)(2,1)} %slice.347), channel_id=1, source_target_pairs={{0,2},{1,3},{2,0},{3,1},{4,6},{5,7},{6,4},{7,5},{8,10},{9,11},{10,... | collective-permute-start | bytes 2359304 | tf_op jit(solution)/shard_map/ppermute | solution.py:33
  185.1 5.3 %copy-start.6 = (bf16[2,8,64,2048]{3,2,1,0:T(8,128)(2,1)S(1)}, bf16[2,8,64,2048]{3,2,1,0:T(8,128)(2,1)}, u32[]{:S(2)}) copy-start(bf16[2,8,64,2048]{3,2,1,0:T(8,128)(2,1)} %shard_map.127) | copy-start | bytes 12582916
  185.1 5.3 %copy-start.11 = (bf16[1,2048,512]{2,1,0:T(8,128)(2,1)S(1)}, bf16[1,2048,512]{2,1,0:T(8,128)(2,1)}, u32[]{:S(2)}) copy-start(bf16[1,2048,512]{2,1,0:T(8,128)(2,1)} %param.22) | copy-start | bytes 6291460
  190.5 2.9 copy-start.8
  194.4 1.6 copy-start.12
  195.9 31.1 %collective-permute-start.9 = (bf16[512,1280]{1,0:T(8,128)(2,1)S(1)}, bf16[512,1280]{1,0:T(8,128)(2,1)S(1)}, u32[]{:S(2)}, u32[]{:S(2)}) collective-permute-start(bf16[512,1280]{1,0:T(8,128)(2,1)S(1)} %copy-done.12), channel_id=1, source_target_pairs={{0,2},{1,3},{2,0},{3,1},{4,6},{5,7},{6,4},{7,5},{8,10},{9,11},{10,... | collective-permute-start | bytes 3932168 | tf_op jit(solution)/shard_map/ppermute | solution.py:33
  207.1 22.8 %collective-permute-start.8 = (bf16[512,768]{1,0:T(8,128)(2,1)S(1)}, bf16[512,768]{1,0:T(8,128)(2,1)S(1)}, u32[]{:S(2)}, u32[]{:S(2)}) collective-permute-start(bf16[512,768]{1,0:T(8,128)(2,1)S(1)} %slice.349), channel_id=1, source_target_pairs={{0,1},{1,0},{2,3},{3,2},{4,5},{5,4},{6,7},{7,6},{8,9},{9,8},{10,11... | collective-permute-start | bytes 2359304 | tf_op jit(solution)/shard_map/ppermute | solution.py:33
  228.6 2.4 copy-start.3
  229.9 25.6 %collective-permute-start.10 = (bf16[512,1280]{1,0:T(8,128)(2,1)}, bf16[512,1280]{1,0:T(8,128)(2,1)}, u32[]{:S(2)}, u32[]{:S(2)}) collective-permute-start(bf16[512,1280]{1,0:T(8,128)(2,1)} %slice.352), channel_id=1, source_target_pairs={{0,1},{1,0},{2,3},{3,2},{4,5},{5,4},{6,7},{7,6},{8,9},{9,8},{10,11... | collective-permute-start | bytes 3932168 | tf_op jit(solution)/shard_map/ppermute | solution.py:33
  252.5 3.0 %copy-start.4 = (bf16[1024,1280]{1,0:T(8,128)(2,1)S(1)}, bf16[1024,1280]{1,0:T(8,128)(2,1)}, u32[]{:S(2)}) copy-start(bf16[1024,1280]{1,0:T(8,128)(2,1)} %copy-done.3) | copy-start | bytes 7864324
  290.4 1.8 copy-start.2
  292.5 0.8 copy-start.15
  292.8 1.7 copy-start.1
